TPU v7x, 256 devices: a 8x8x2 block of a 8x8x16 slice. The times are simulated.
256 devices in a mesh: grp: 2 (over z), sp: 16 (over y, core), tp: 8 (over x).
Axes of the slice: x: 8, y: 8, z: 2, core: 2. Of those that a mesh axis runs over, the one named last changes fastest.
The devices are a block of a 8x8x16 slice.
Arguments:
- resid_in: bfloat16 [32768, 2048], P(('grp', 'sp', 'tp')), parts along dimension 0, may hold values from -6 to 6
- pool_input: bfloat16 [32768, 1024], P(('grp', 'sp'), 'tp'), parts along dimension 0, may hold values from -6 to 6
- pool_weight: bfloat16 [4, 256, 256], replicated, may hold values from -0.375 to 0.375
- pool_scale: float32 [1024], replicated, may hold values from 0.2 to 0.8
- out_weight: bfloat16 [1024, 2048], replicated, may hold values from -0.1875 to 0.1875
- mix_gain: float32 [2048], replicated, may hold values from 0.1 to 1.9
- ffn_gain: float32 [2048], replicated, may hold values from 0.1 to 1.9
- w_gate: bfloat16 [32, 2048, 1024], P('sp', None, 'tp'), may hold values from -0.375 to 0.375
- w_up: bfloat16 [32, 2048, 1024], P('sp', None, 'tp'), may hold values from -0.375 to 0.375
- w_down: bfloat16 [32, 1024, 2048], P('sp', 'tp'), may hold values from -0.1875 to 0.1875
- routes: int32 [32768, 2], P(('grp', 'sp', 'tp')), parts along dimension 0, may hold values from 0 to 31, all different within a row; in each aligned block of 128 rows (0 to 127, 128 to 255, ...) at most 9 rows name the same one
- route_weight: float32 [32768, 2], P(('grp', 'sp', 'tp')), parts along dimension 0, may hold values from 0.1 to 1
- post_gain: float32 [2048], replicated, may hold values from 0.1 to 1.9
Outputs:
- layer_out: bfloat16 [32768, 2048], P(('grp', 'sp', 'tp')), parts along dimension 0
There are 2 independent parts, one for each index of `grp`. A program takes and returns all parts, laid end to end along the dimension named above; an argument that names none is the same for every part. Nothing has to cross between parts.
Inputs may be any that keep to these rules, and one draw needn't show every extreme that they name: `routes`: each row names 2 different experts. The rows of one device name any one expert at most 9 times, and in every draw some device's rows name some expert exactly 9 times.
All inputs are finite; a program needn't handle non-finite values.
Results may differ from a plain program's by a relative error of at most 0.011.
Values may be sent and summed in bfloat16 or wider, within the bound.
A program may use at most 128 MiB of HBM per device.

v0:
```python
import jax
import jax.numpy as jnp
from jax import lax
from jax.sharding import PartitionSpec as P

GROUPS = 4
GROUP_DIM = 256
TOP = 2
CAP = 9
pool_windows = (2, 4, 8, 16)
reach_back = 15
norm_eps = 1e-06
clamp_limit = 7.0
glu_alpha = 1.702


def passed_along(x, axis, by):
    size = lax.axis_size(axis)
    pairs = [(i, i + by) for i in range(size) if 0 <= i + by < size]
    return lax.ppermute(x, axis, pairs)


def rms_scale(values, gain_vec):
    inverse = lax.rsqrt(jnp.mean(values * values, axis=-1, keepdims=True) + norm_eps)
    return values * inverse * gain_vec


def clamped_unit(gate_pre, upward):
    gate_clip = jnp.minimum(gate_pre, clamp_limit)
    linear = jnp.clip(upward, -clamp_limit, clamp_limit)
    return gate_clip * jax.nn.sigmoid(glu_alpha * gate_clip) * (linear + 1.0)


def per_device(
    resid_in,
    pool_input,
    pool_weight,
    pool_scale,
    out_weight,
    mix_gain,
    ffn_gain,
    w_gate,
    w_up,
    w_down,
    routes,
    route_weight,
    post_gain,
):
    n_sp = lax.axis_size("sp")
    n_tp = lax.axis_size("tp")
    seg_rows, channels = pool_input.shape
    last_rows = pool_input[seg_rows - reach_back :]
    before = passed_along(last_rows, "sp", 1)
    extended = jnp.concatenate([before, pool_input], axis=0).astype(jnp.float32)
    first_chan = lax.axis_index("tp") * channels
    chan_group = (first_chan + lax.iota(jnp.int32, channels)) // GROUP_DIM
    positions = lax.axis_index("sp") * seg_rows + lax.iota(jnp.int32, seg_rows)
    window = jnp.zeros((channels,), jnp.int32)
    for group_level, win_len in enumerate(pool_windows):
        window = jnp.where(chan_group == group_level, win_len, window)
    running = jnp.zeros((seg_rows, channels), jnp.float32)
    window_sum = running
    for offset in range(pool_windows[-1]):
        running = running + extended[reach_back - offset : reach_back - offset + seg_rows]
        if offset + 1 in pool_windows:
            window_sum = jnp.where(window[None, :] == offset + 1, running, window_sum)
    divisor = jnp.minimum(positions[:, None] + 1, window[None, :]).astype(jnp.float32)
    mixed_rows = (window_sum / divisor - extended[reach_back:]).astype(jnp.bfloat16)
    token_mixed = lax.all_to_all(mixed_rows, "tp", split_axis=0, concat_axis=1, tiled=True)
    tok_rows = token_mixed.shape[0]
    pooled = jnp.einsum(
        "tgc,gcd->tgd",
        token_mixed.reshape(tok_rows, GROUPS, GROUP_DIM),
        pool_weight,
        preferred_element_type=jnp.float32,
    )
    pooled = (
        (pooled * pool_scale.reshape(GROUPS, GROUP_DIM)).astype(jnp.bfloat16).reshape(tok_rows, -1)
    )
    mix_out = jnp.dot(pooled, out_weight, preferred_element_type=jnp.float32)
    residual = (resid_in.astype(jnp.float32) + rms_scale(mix_out, mix_gain)).astype(jnp.bfloat16)
    normed = rms_scale(residual.astype(jnp.float32), ffn_gain).astype(jnp.bfloat16)
    width = normed.shape[1]
    local_experts = w_gate.shape[0]
    n_experts = local_experts * n_sp
    slot_total = n_experts * CAP
    flat_route = routes.reshape(-1)
    onehot = (flat_route[:, None] == lax.iota(jnp.int32, n_experts)[None, :]).astype(jnp.int32)
    slot_rank = jnp.sum((jnp.cumsum(onehot, axis=0) - onehot) * onehot, axis=1)
    slot_index = flat_route * CAP + slot_rank
    picker = slot_index[:, None] == lax.iota(jnp.int32, slot_total)[None, :]
    picker_rows = picker.astype(jnp.bfloat16)
    token_pick = jnp.sum(
        picker.reshape(tok_rows, TOP, slot_total).astype(jnp.float32), axis=1
    ).astype(jnp.bfloat16)
    buffer = lax.dot_general(
        token_pick, normed, (((0,), (0,)), ((), ())), preferred_element_type=jnp.float32
    )
    outgoing = buffer.astype(jnp.bfloat16).reshape(n_sp, local_experts * CAP, width)
    at_owner = lax.all_to_all(outgoing, "sp", split_axis=0, concat_axis=0, tiled=True)
    arrived = lax.all_gather(at_owner[:, None], "tp", axis=1, tiled=True)
    arrived = arrived.reshape(n_sp, n_tp, local_experts, CAP, width)
    gate_pre = jnp.einsum("sklcd,ldf->sklcf", arrived, w_gate, preferred_element_type=jnp.float32)
    upward = jnp.einsum("sklcd,ldf->sklcf", arrived, w_up, preferred_element_type=jnp.float32)
    activated = clamped_unit(gate_pre, upward).astype(jnp.bfloat16)
    terms = jnp.einsum("sklcf,lfd->kslcd", activated, w_down, preferred_element_type=jnp.float32)
    summed = lax.psum_scatter(
        terms.reshape(1 * lax.axis_size("tp"), n_sp, local_experts * CAP, width).astype(
            jnp.bfloat16
        ),
        "tp",
        scatter_dimension=0,
        tiled=True,
    ).astype(jnp.float32)
    results = summed[0].astype(jnp.bfloat16)
    returned = lax.all_to_all(results, "sp", split_axis=0, concat_axis=0, tiled=True).reshape(
        slot_total, width
    )
    gathered = jnp.dot(picker_rows, returned, preferred_element_type=jnp.float32)
    expert_mix = jnp.sum(gathered.reshape(tok_rows, TOP, width) * route_weight[:, :, None], axis=1)
    return (residual.astype(jnp.float32) + rms_scale(expert_mix, post_gain)).astype(jnp.bfloat16)


def solution(mesh):
    in_specs = (
        P(("grp", "sp", "tp"), None),
        P(("grp", "sp"), "tp"),
        P(),
        P(),
        P(),
        P(),
        P(),
        P("sp", None, "tp"),
        P("sp", None, "tp"),
        P("sp", "tp", None),
        P(("grp", "sp", "tp"), None),
        P(("grp", "sp", "tp"), None),
        P(),
    )
    out_specs = P(("grp", "sp", "tp"), None)
    return jax.shard_map(
        per_device, mesh=mesh, in_specs=in_specs, out_specs=out_specs, check_vma=False
    )
```

profile of v0, /device:TPU:513, one launch (start us, length us, event | category | flops | bytes accessed | tf_op | source)
XLA Modules:
  0.0 397.1 jit_solution(8766756153125260866)
XLA Ops:
  6.6 0.8 slice.58
  7.3 5.7 %collective-permute-start = (bf16[15,128]{1,0:T(8,128)(2,1)S(1)}, bf16[15,128]{1,0:T(8,128)(2,1)S(1)}, u32[]{:S(2)}, u32[]{:S(2)}) collective-permute-start(bf16[15,128]{1,0:T(8,128)(2,1)S(1)} %slice.58), channel_id=1, source_target_pairs={{0,8},{8,16},{16,24},{24,32},{32,40},{40,48},{48,56},{56,64},{64,7... | collective-permute-start | bytes 11528 | tf_op jit(solution)/shard_map/ppermute | solution.py:20
  13.1 0.8 copy.76
  13.9 0.1 eq.194
  14.1 0.6 reduce-window.6
  14.7 15.0 %collective-permute-done = bf16[15,128]{1,0:T(8,128)(2,1)S(1)} collective-permute-done((bf16[15,128]{1,0:T(8,128)(2,1)S(1)}, bf16[15,128]{1,0:T(8,128)(2,1)S(1)}, u32[]{:S(2)}, u32[]{:S(2)}) %collective-permute-start) | collective-permute-done | bytes 3872 | tf_op jit(solution)/shard_map/ppermute | solution.py:20
  29.7 1.0 maximum_convert_fusion
  30.7 0.0 copy-start.7
  30.7 0.0 copy-start.6
  30.7 1.5 fusion.42
  32.2 3.7 all-to-all-start
  36.0 0.1 all-gather.3.cloned.1.call-start
  36.0 0.2 slice_reduce_fusion
  36.2 0.1 eq.190
  36.4 0.1 fusion.49
  36.5 0.1 reduce_sum.58
  36.7 0.1 copy.79
  36.7 0.1 convert_reduce_fusion
  36.8 9.4 %all-to-all-done = bf16[8,128,128]{2,1,0:T(8,128)(2,1)S(1)} async-done(((bf16[8,128,128]{2,1,0:T(8,128)(2,1)}), bf16[8,128,128]{2,1,0:T(8,128)(2,1)S(1)}, u32[]{:S(2)}, u32[]{:S(2)}) %all-to-all-start) | async-done | bytes 262176 | tf_op jit(solution)/shard_map/all_to_all | solution.py:69
  46.2 0.2 copy.73
  46.4 0.3 fusion.27
  46.7 0.2 copy.75
  46.9 0.0 copy-start.2
  46.9 0.0 copy-start.3
  46.9 3.1 multiply_reduce_fusion.1
  50.0 0.4 fusion.28
  50.4 0.3 copy-done.4
  50.7 1.6 convolution_convert_fusion
  52.2 1.4 reshape.162
  53.7 44.4 %all_to_all.26 = bf16[16,18,2048]{2,1,0:T(8,128)(2,1)S(1)} all-to-all(bf16[16,18,2048]{2,1,0:T(8,128)(2,1)S(1)} %reshape.162), channel_id=1, replica_groups=mesh['grp'=2,'sp'=16,'tp'=8] {'sp'}, dimensions={0} | all-to-all | bytes 2359296 | tf_op jit(solution)/shard_map/all_to_all | solution.py:100
  98.1 1.7 copy.80
  99.8 0.1 all-gather.3.cloned.1.call-update
  99.8 0.2 reduce-scatter.2.cloned.1.call-start
  100.1 104.1 %all-gather.3.cloned.1.call-done = bf16[16,144,2048]{2,0,1:T(8,128)(2,1)} async-done(((bf16[16,18,2048]{2,0,1:T(8,128)(2,1)}), bf16[16,144,2048]{2,0,1:T(8,128)(2,1)}) %all-gather.3.cloned.1.call-update) | async-done | bytes 9437200 | tf_op jit(solution)/shard_map/all_gather | solution.py:101
  204.2 5.3 %fusion.20 = f32[16,8,2,9,128]{4,0,3,1,2:T(8,128)S(1)} fusion(bf16[16,8,2,9,2048]{4,0,3,2,1:T(8,128)(2,1)} %bitcast.67, bf16[2,2048,128]{2,1,0:T(8,128)(2,1)S(1)} %copy-done.9), kind=kOutput, calls=%fused_computation.16 | convolution fusion | flops 1208254464 | bytes 11665408 | tf_op jit(solution)/shard_map/sklcd,ldf->sklcf/dot_general | solution.py:103
  209.5 1.1 copy-done.8
  210.6 0.2 copy-done.10
  210.9 2.8 fusion.23
  213.7 5.1 %convert_bitcast_fusion = bf16[8,16,2,9,2048]{4,0,3,1,2:T(8,128)(2,1)} fusion(bf16[2,128,2048]{2,1,0:T(8,128)(2,1)S(1)} %copy-done, bf16[16,8,2,9,128]{4,0,3,1,2:T(8,128)(2,1)S(1)} %fusion.23), kind=kOutput, calls=%fused_computation | convolution fusion | flops 1212678144 | bytes 11075584 | tf_op jit(solution)/shard_map/sklcf,lfd->kslcd/dot_general | solution.py:106
  218.8 12.5 %copy.84 = bf16[8,16,2,9,2048]{4,1,3,2,0:T(8,128)(2,1)} copy(bf16[8,16,2,9,2048]{4,0,3,1,2:T(8,128)(2,1)} %convert_bitcast_fusion) | data formatting | bytes 18874368 | tf_op jit(solution)/shard_map/convert_element_type | solution.py:108
  231.3 0.1 reduce-scatter.2.cloned.1.call-update
  231.3 105.1 %reduce-scatter.2.cloned.1.call-done = bf16[1,16,18,2048]{3,1,2,0:T(8,128)(2,1)} async-done(((bf16[8,16,18,2048]{3,1,2,0:T(8,128)(2,1)}), bf16[1,16,18,2048]{3,1,2,0:T(8,128)(2,1)}) %reduce-scatter.2.cloned.1.call-update) | async-done | bytes 1179664 | tf_op jit(solution)/shard_map/reduce_scatter | solution.py:107
  336.5 2.0 copy.85
  338.5 47.2 %all_to_all.27 = bf16[16,18,2048]{2,1,0:T(8,128)(2,1)S(1)} all-to-all(bf16[16,18,2048]{2,1,0:T(8,128)(2,1)S(1)} %copy.85), channel_id=1, replica_groups=mesh['grp'=2,'sp'=16,'tp'=8] {'sp'}, dimensions={0} | all-to-all | bytes 2359296 | tf_op jit(solution)/shard_map/all_to_all | solution.py:116
  385.7 1.2 reshape.170
  386.9 2.1 fusion.4
  389.0 0.2 multiply_reduce_fusion
  389.2 1.0 fusion.31
  (29 shorter events, 0.2 us)
Async XLA Ops:
  6.5 207.2 %copy-start = (bf16[2,128,2048]{2,1,0:T(8,128)(2,1)S(1)}, bf16[2,128,2048]{2,1,0:T(8,128)(2,1)}, u32[]{:S(2)}) copy-start(bf16[2,128,2048]{2,1,0:T(8,128)(2,1)} %param.22) | copy-start | bytes 3145732
  7.3 22.4 %collective-permute-start = (bf16[15,128]{1,0:T(8,128)(2,1)S(1)}, bf16[15,128]{1,0:T(8,128)(2,1)S(1)}, u32[]{:S(2)}, u32[]{:S(2)}) collective-permute-start(bf16[15,128]{1,0:T(8,128)(2,1)S(1)} %slice.58), channel_id=1, source_target_pairs={{0,8},{8,16},{16,24},{24,32},{32,40},{40,48},{48,56},{56,64},{64,7... | collective-permute-start | bytes 11528 | tf_op jit(solution)/shard_map/ppermute | solution.py:20
  30.7 5.7 %copy-start.7 = (f32[1024]{0:T(1024)S(1)}, f32[1024]{0:T(1024)}, u32[]{:S(2)}) copy-start(f32[1024]{0:T(1024)} %param.16) | copy-start | bytes 12292
  30.7 6.0 %copy-start.6 = (s32[128,2]{0,1:T(2,128)S(1)}, s32[128,2]{0,1:T(2,128)}, u32[]{:S(2)}) copy-start(s32[128,2]{0,1:T(2,128)} %param.23) | copy-start | bytes 3076
  32.2 14.2 %copy-start.1 = (bf16[4,256,256]{2,1,0:T(8,128)(2,1)S(1)}, bf16[4,256,256]{2,1,0:T(8,128)(2,1)}, u32[]{:S(2)}) copy-start(bf16[4,256,256]{2,1,0:T(8,128)(2,1)} %param.15) | copy-start | bytes 1572868
  32.2 14.0 %all-to-all-start = ((bf16[8,128,128]{2,1,0:T(8,128)(2,1)}), bf16[8,128,128]{2,1,0:T(8,128)(2,1)S(1)}, u32[]{:S(2)}, u32[]{:S(2)}) async-start(bf16[8,128,128]{2,1,0:T(8,128)(2,1)} %bitcast), calls=%async_computation | async-start | bytes 524288 | tf_op jit(solution)/shard_map/all_to_all | solution.py:69
  36.0 168.2 %all-gather.3.cloned.1.call-start = ((), (), s32[]{:S(2)}) async-start(), calls=%async_computation.5 | async-start | bytes 10616832 | tf_op jit(solution)/shard_map/all_gather | solution.py:101
  46.9 3.1 copy-start.2
  46.9 3.1 copy-start.3
  50.0 0.7 copy-start.4
  99.8 104.4 %copy-start.9 = (bf16[2,2048,128]{2,1,0:T(8,128)(2,1)S(1)}, bf16[2,2048,128]{2,1,0:T(8,128)(2,1)}, u32[]{:S(2)}) copy-start(bf16[2,2048,128]{2,1,0:T(8,128)(2,1)} %param.20) | copy-start | bytes 3145732
  99.8 236.6 %reduce-scatter.2.cloned.1.call-start = ((), (), s32[]{:S(2)}) async-start(), calls=%async_computation.4 | async-start | bytes 10616832 | tf_op jit(solution)/shard_map/reduce_scatter | solution.py:107
  204.2 6.4 %copy-start.8 = (bf16[16,144,2048]{2,0,1:T(8,128)(2,1)S(1)}, bf16[16,144,2048]{2,0,1:T(8,128)(2,1)}, u32[]{:S(2)}) copy-start(bf16[16,144,2048]{2,0,1:T(8,128)(2,1)} %all-gather.3.cloned.1.call-done) | copy-start | bytes 28311556
  204.2 6.7 %copy-start.10 = (bf16[2,2048,128]{2,1,0:T(8,128)(2,1)S(1)}, bf16[2,2048,128]{2,1,0:T(8,128)(2,1)}, u32[]{:S(2)}) copy-start(bf16[2,2048,128]{2,1,0:T(8,128)(2,1)} %param.21) | copy-start | bytes 3145732
  385.7 1.2 copy-start.11
  386.9 2.3 copy-start.5
Sparse Core Ops, SparseCore 0:
  100.0 104.1 all-gather.2
  231.5 104.9 reduce-scatter.1
where the time goes:
time: 398 us; the launch traced here: 397 us
  waiting for transfers between devices  234 us (59%)
  blocking collectives  91.7 us (23%)
  local copies, waits for them, and re-layouts  23 us (6%)
  matrix products  20.2 us (5%)
  between operations  13.7 us (3%)
  starting transfers between devices  9.79 us (2%)
  other arithmetic  4.91 us (1%)
    reduce_scatter x1, waiting for transfers between devices, per_device(): lax.psum_scatter(terms.reshape(1 * lax.axis_size('tp'), n_sp, local_exper...  105 us
    all_gather x1, waiting for transfers between devices, per_device(): arrived = lax.all_gather(at_owner[:, None], 'tp', axis=1, tiled=True)  104 us
    all_to_all x1, blocking collectives, per_device(): lax.all_to_all(results, 'sp', split_axis=0, concat_axis=0, tiled=True)  47.2 us
    all_to_all x1, blocking collectives, per_device(): lax.all_to_all(outgoing, 'sp', split_axis=0, concat_axis=0, tiled=True)  44.4 us
    ppermute x1, waiting for transfers between devices, passed_along(): return lax.ppermute(x, axis, pairs)  15 us
    convert_element_type x1, local copies, waits for them, and re-layouts, per_device(): terms.reshape(1 * lax.axis_size('tp'), n_sp, local_experts * CAP, width)  12.5 us
    all_to_all x1, waiting for transfers between devices, per_device(): lax.all_to_all(mixed_rows, 'tp', split_axis=0, concat_axis=1, tiled=True)  9.42 us
  transfers between devices with their start and end apart: 4, of which 4 were waited for; matrix products, arithmetic and copies ran while one was open for 1% of the time, Pallas kernels for 0%

commit v1 on v0

--- a/solution.py
+++ b/solution.py
@@ -98,7 +98,9 @@
     )
     outgoing = buffer.astype(jnp.bfloat16).reshape(n_sp, local_experts * CAP, width)
     at_owner = lax.all_to_all(outgoing, "sp", split_axis=0, concat_axis=0, tiled=True)
-    arrived = lax.all_gather(at_owner[:, None], "tp", axis=1, tiled=True)
+    block = at_owner[:, None]
+    sent = jnp.stack([block] * lax.axis_size("tp"))
+    arrived = jnp.concatenate(lax.all_to_all(sent, "tp", 0, 0), axis=1)
     arrived = arrived.reshape(n_sp, n_tp, local_experts, CAP, width)
     gate_pre = jnp.einsum("sklcd,ldf->sklcf", arrived, w_gate, preferred_element_type=jnp.float32)
     upward = jnp.einsum("sklcd,ldf->sklcf", arrived, w_up, preferred_element_type=jnp.float32)

time: 398 us -> 525 us (1.32)
  blocking collectives: 91.7 us -> 304 us
  waiting for transfers between devices: 234 us -> 131 us
  matrix products: 20.2 us -> 39.3 us
    all_to_all x0 -> x1, blocking collectives: none -> 212 us  [per_device(): arrived = jnp.concatenate(lax.all_to_all(sent, 'tp', 0, 0), axis=1)]
    all_gather x1 -> x0, waiting for transfers between devices: 104 us -> none  [per_device(): arrived = lax.all_gather(at_owner[:, None], 'tp', axis=1, tiled=True)]
    dot_general x1, matrix products: 2.82 us -> 15.7 us  [per_device(): jnp.einsum('sklcd,ldf->sklcf', arrived, w_up, preferred_element_type=jnp....]
    dot_general x1, matrix products: 5.33 us -> 11.3 us  [per_device(): jnp.einsum('sklcd,ldf->sklcf', arrived, w_gate, preferred_element_type=jn...]
  transfers between devices with their start and end apart: 4 -> 3, of which waited for: 4 -> 3; matrix products, arithmetic and copies ran while one was open for 1% -> 0% of each run, Pallas kernels for 0% -> 0%
where the time goes in v1:
time: 525 us; the launch traced here: 524 us
  blocking collectives  304 us (58%)
  waiting for transfers between devices  131 us (25%)
  matrix products  39.3 us (7%)
  local copies, waits for them, and re-layouts  21.9 us (4%)
  between operations  13.7 us (3%)
  starting transfers between devices  9.55 us (2%)
  other arithmetic  5.53 us (1%)
    all_to_all x1, blocking collectives, per_device(): arrived = jnp.concatenate(lax.all_to_all(sent, 'tp', 0, 0), axis=1)  212 us
    reduce_scatter x1, waiting for transfers between devices, per_device(): lax.psum_scatter(terms.reshape(1 * lax.axis_size('tp'), n_sp, local_exper...  106 us
    all_to_all x1, blocking collectives, per_device(): lax.all_to_all(results, 'sp', split_axis=0, concat_axis=0, tiled=True)  47.2 us
    all_to_all x1, blocking collectives, per_device(): lax.all_to_all(outgoing, 'sp', split_axis=0, concat_axis=0, tiled=True)  44.4 us
    dot_general x1, matrix products, per_device(): jnp.einsum('sklcd,ldf->sklcf', arrived, w_up, preferred_element_type=jnp....  15.7 us
    ppermute x1, waiting for transfers between devices, passed_along(): return lax.ppermute(x, axis, pairs)  15 us
    convert_element_type x1, local copies, waits for them, and re-layouts, per_device(): terms.reshape(1 * lax.axis_size('tp'), n_sp, local_experts * CAP, width)  12.5 us
    dot_general x1, matrix products, per_device(): jnp.einsum('sklcd,ldf->sklcf', arrived, w_gate, preferred_element_type=jn...  11.3 us
  transfers between devices with their start and end apart: 3, of which 3 were waited for; matrix products, arithmetic and copies ran while one was open for 0% of the time, Pallas kernels for 0%

profile of v1, /device:TPU:513, one launch (start us, length us, event | category | flops | bytes accessed | tf_op | source)
XLA Modules:
  0.0 524.2 jit_solution(4070096951398227373)
XLA Ops:
  6.6 0.8 slice.58
  7.3 5.7 %collective-permute-start = (bf16[15,128]{1,0:T(8,128)(2,1)S(1)}, bf16[15,128]{1,0:T(8,128)(2,1)S(1)}, u32[]{:S(2)}, u32[]{:S(2)}) collective-permute-start(bf16[15,128]{1,0:T(8,128)(2,1)S(1)} %slice.58), channel_id=1, source_target_pairs={{0,8},{8,16},{16,24},{24,32},{32,40},{40,48},{48,56},{56,64},{64,7... | collective-permute-start | bytes 11528 | tf_op jit(solution)/shard_map/ppermute | solution.py:20
  13.1 0.8 copy.89
  13.9 0.1 eq.194
  14.1 0.6 reduce-window.6
  14.7 15.0 %collective-permute-done = bf16[15,128]{1,0:T(8,128)(2,1)S(1)} collective-permute-done((bf16[15,128]{1,0:T(8,128)(2,1)S(1)}, bf16[15,128]{1,0:T(8,128)(2,1)S(1)}, u32[]{:S(2)}, u32[]{:S(2)}) %collective-permute-start) | collective-permute-done | bytes 3872 | tf_op jit(solution)/shard_map/ppermute | solution.py:20
  29.7 1.0 maximum_convert_fusion
  30.7 0.0 copy-start.8
  30.7 0.0 copy-start.7
  30.7 1.5 fusion.27
  32.2 3.7 all-to-all-start
  36.0 0.1 reduce-scatter.2.cloned.1.call-start
  36.0 0.2 slice_reduce_fusion
  36.2 0.1 eq.190
  36.4 0.1 fusion.34
  36.5 0.1 reduce_sum.58
  36.7 0.1 copy.92
  36.7 0.1 convert_reduce_fusion
  36.8 9.4 %all-to-all-done = bf16[8,128,128]{2,1,0:T(8,128)(2,1)S(1)} async-done(((bf16[8,128,128]{2,1,0:T(8,128)(2,1)}), bf16[8,128,128]{2,1,0:T(8,128)(2,1)S(1)}, u32[]{:S(2)}, u32[]{:S(2)}) %all-to-all-start) | async-done | bytes 262176 | tf_op jit(solution)/shard_map/all_to_all | solution.py:69
  46.2 0.2 copy.86
  46.4 0.3 fusion.12
  46.7 0.2 copy.88
  46.9 0.0 copy-start.3
  46.9 0.0 copy-start.4
  46.9 3.1 multiply_reduce_fusion.1
  50.0 0.0 copy-start.5
  50.0 0.4 fusion.13
  50.4 0.3 copy-done.5
  50.7 1.6 convolution_convert_fusion
  52.2 1.4 reshape.164
  53.7 44.4 %all_to_all.31 = bf16[16,18,2048]{2,1,0:T(8,128)(2,1)S(1)} all-to-all(bf16[16,18,2048]{2,1,0:T(8,128)(2,1)S(1)} %reshape.164), channel_id=1, replica_groups=mesh['grp'=2,'sp'=16,'tp'=8] {'sp'}, dimensions={0} | all-to-all | bytes 2359296 | tf_op jit(solution)/shard_map/all_to_all | solution.py:100
  98.1 0.7 copy.93
  98.8 1.2 stack.3
  100.0 0.0 copy-start.9
  100.0 212.1 %all_to_all.32 = bf16[8,16,1,18,2048]{4,1,3,2,0:T(8,128)(2,1)} all-to-all(bf16[8,16,1,18,2048]{4,1,3,2,0:T(8,128)(2,1)S(1)} %stack.3), channel_id=1, replica_groups=mesh['grp'=2,'sp'=16,'tp'=8] {'tp'}, dimensions={0} | all-to-all | bytes 18874368 | tf_op jit(solution)/shard_map/all_to_all | solution.py:103
  312.0 15.7 %fusion = f32[2,16,8,9,128]{4,2,3,1,0:T(8,128)S(1)} fusion(bf16[16,8,2,9,2048]{4,0,3,2,1:T(8,128)(2,1)} %bitcast.78, bf16[2,2048,128]{2,1,0:T(8,128)(2,1)S(1)} %copy-done.9), kind=kOutput, calls=%fused_computation.1 | convolution fusion | flops 1207959552 | bytes 11665408 | tf_op jit(solution)/shard_map/sklcd,ldf->sklcf/dot_general | solution.py:106
  327.7 11.3 %fusion.2 = f32[2,16,8,9,128]{4,2,3,1,0:T(8,128)S(1)} fusion(bf16[16,8,2,9,2048]{4,0,3,2,1:T(8,128)(2,1)S(1)} %bitcast.79, bf16[2,2048,128]{2,1,0:T(8,128)(2,1)} %param.20), kind=kOutput, calls=%fused_computation.3 | convolution fusion | flops 1207959552 | bytes 11665408 | tf_op jit(solution)/shard_map/sklcd,ldf->sklcf/dot_general | solution.py:105
  339.1 0.6 fusion.6
  339.7 5.3 %convert_bitcast_fusion = bf16[8,16,2,9,2048]{4,0,3,1,2:T(8,128)(2,1)} fusion(bf16[2,128,2048]{2,1,0:T(8,128)(2,1)S(1)} %copy-done, bf16[16,8,2,9,128]{4,0,3,1,2:T(8,128)(2,1)S(1)} %fusion.6), kind=kOutput, calls=%fused_computation | convolution fusion | flops 1212678144 | bytes 11075584 | tf_op jit(solution)/shard_map/sklcf,lfd->kslcd/dot_general | solution.py:108
  345.0 12.5 %copy.98 = bf16[8,16,2,9,2048]{4,1,3,2,0:T(8,128)(2,1)} copy(bf16[8,16,2,9,2048]{4,0,3,1,2:T(8,128)(2,1)} %convert_bitcast_fusion) | data formatting | bytes 18874368 | tf_op jit(solution)/shard_map/convert_element_type | solution.py:110
  357.5 0.1 reduce-scatter.2.cloned.1.call-update
  357.6 106.1 %reduce-scatter.2.cloned.1.call-done = bf16[1,16,18,2048]{3,1,2,0:T(8,128)(2,1)} async-done(((bf16[8,16,18,2048]{3,1,2,0:T(8,128)(2,1)}), bf16[1,16,18,2048]{3,1,2,0:T(8,128)(2,1)}) %reduce-scatter.2.cloned.1.call-update) | async-done | bytes 1179664 | tf_op jit(solution)/shard_map/reduce_scatter | solution.py:109
  463.6 2.0 copy.99
  465.6 47.2 %all_to_all.33 = bf16[16,18,2048]{2,1,0:T(8,128)(2,1)S(1)} all-to-all(bf16[16,18,2048]{2,1,0:T(8,128)(2,1)S(1)} %copy.99), channel_id=1, replica_groups=mesh['grp'=2,'sp'=16,'tp'=8] {'sp'}, dimensions={0} | all-to-all | bytes 2359296 | tf_op jit(solution)/shard_map/all_to_all | solution.py:118
  512.8 1.2 reshape.170
  514.0 2.1 fusion.4
  516.1 0.2 multiply_reduce_fusion
  516.3 1.0 fusion.16
  (27 shorter events, 0.2 us)
Async XLA Ops:
  6.5 333.1 %copy-start = (bf16[2,128,2048]{2,1,0:T(8,128)(2,1)S(1)}, bf16[2,128,2048]{2,1,0:T(8,128)(2,1)}, u32[]{:S(2)}) copy-start(bf16[2,128,2048]{2,1,0:T(8,128)(2,1)} %param.22) | copy-start | bytes 3145732
  7.3 22.4 %collective-permute-start = (bf16[15,128]{1,0:T(8,128)(2,1)S(1)}, bf16[15,128]{1,0:T(8,128)(2,1)S(1)}, u32[]{:S(2)}, u32[]{:S(2)}) collective-permute-start(bf16[15,128]{1,0:T(8,128)(2,1)S(1)} %slice.58), channel_id=1, source_target_pairs={{0,8},{8,16},{16,24},{24,32},{32,40},{40,48},{48,56},{56,64},{64,7... | collective-permute-start | bytes 11528 | tf_op jit(solution)/shard_map/ppermute | solution.py:20
  30.7 5.7 %copy-start.8 = (f32[1024]{0:T(1024)S(1)}, f32[1024]{0:T(1024)}, u32[]{:S(2)}) copy-start(f32[1024]{0:T(1024)} %param.16) | copy-start | bytes 12292
  30.7 6.0 %copy-start.7 = (s32[128,2]{0,1:T(2,128)S(1)}, s32[128,2]{0,1:T(2,128)}, u32[]{:S(2)}) copy-start(s32[128,2]{0,1:T(2,128)} %param.23) | copy-start | bytes 3076
  32.2 14.2 %copy-start.2 = (bf16[4,256,256]{2,1,0:T(8,128)(2,1)S(1)}, bf16[4,256,256]{2,1,0:T(8,128)(2,1)}, u32[]{:S(2)}) copy-start(bf16[4,256,256]{2,1,0:T(8,128)(2,1)} %param.15) | copy-start | bytes 1572868
  32.2 14.0 %all-to-all-start = ((bf16[8,128,128]{2,1,0:T(8,128)(2,1)}), bf16[8,128,128]{2,1,0:T(8,128)(2,1)S(1)}, u32[]{:S(2)}, u32[]{:S(2)}) async-start(bf16[8,128,128]{2,1,0:T(8,128)(2,1)} %bitcast), calls=%async_computation | async-start | bytes 524288 | tf_op jit(solution)/shard_map/all_to_all | solution.py:69
  36.0 427.7 %reduce-scatter.2.cloned.1.call-start = ((), (), s32[]{:S(2)}) async-start(), calls=%async_computation.5 | async-start | bytes 10616832 | tf_op jit(solution)/shard_map/reduce_scatter | solution.py:109
  46.9 3.1 copy-start.3
  46.9 3.1 copy-start.4
  50.0 0.7 copy-start.5
  100.0 212.1 %copy-start.9 = (bf16[2,2048,128]{2,1,0:T(8,128)(2,1)S(1)}, bf16[2,2048,128]{2,1,0:T(8,128)(2,1)}, u32[]{:S(2)}) copy-start(bf16[2,2048,128]{2,1,0:T(8,128)(2,1)} %param.21) | copy-start | bytes 3145732
  312.0 15.7 %copy-start.1 = (bf16[8,16,1,18,2048]{4,1,3,2,0:T(8,128)(2,1)S(1)}, bf16[8,16,1,18,2048]{4,1,3,2,0:T(8,128)(2,1)}, u32[]{:S(2)}) copy-start(bf16[8,16,1,18,2048]{4,1,3,2,0:T(8,128)(2,1)} %all_to_all.32) | copy-start | bytes 28311556
  512.8 1.2 copy-start.10
  514.0 2.3 copy-start.6
Sparse Core Ops, SparseCore 0:
  357.7 105.8 reduce-scatter.1
